TPU v7x, 128 devices: a whole 4x4x4 slice. The times are simulated.
128 devices in a mesh: sp: 64 (over z, y, x), tp: 2 (over core).
Axes of the slice: x: 4, y: 4, z: 4, core: 2. Of those that a mesh axis runs over, the one named last changes fastest.
Arguments:
- stream: bfloat16 [16384, 2048], P(('sp', 'tp')), may hold values from -3 to 3
- query_narrow: bfloat16 [16384, 1024], P('sp', 'tp'), may hold values from -6 to 6
- key_narrow: bfloat16 [16384, 128], P('sp', 'tp'), may hold values from -6 to 6
- value_narrow: bfloat16 [16384, 128], P('sp', 'tp'), may hold values from -6 to 6
- query_broad: bfloat16 [16384, 1024], P('sp', 'tp'), may hold values from -6 to 6
- key_broad: bfloat16 [16384, 256], P('sp', 'tp'), may hold values from -6 to 6
- value_broad: bfloat16 [16384, 256], P('sp', 'tp'), may hold values from -6 to 6
- narrow_query_gain: float32 [64], replicated, may hold values from 1.5 to 9
- narrow_key_gain: float32 [64], replicated, may hold values from 1.5 to 9
- broad_query_gain: float32 [128], replicated, may hold values from 1.5 to 9
- broad_key_gain: float32 [128], replicated, may hold values from 1.5 to 9
- out_weight: bfloat16 [2048, 2048], replicated, may hold values from -0.125 to 0.125
- norm_gain: float32 [2048], replicated, may hold values from 0.1 to 1.9
- gate_weight: bfloat16 [64, 2048, 1024], P('sp', None, 'tp'), may hold values from -0.125 to 0.125
- up_weight: bfloat16 [64, 2048, 1024], P('sp', None, 'tp'), may hold values from -0.125 to 0.125
- down_weight: bfloat16 [64, 1024, 2048], P('sp', 'tp'), may hold values from -0.1875 to 0.1875
- route_ids: int32 [16384, 2], P(('sp', 'tp')), may hold values from 0 to 63, all different within a row; in each aligned block of 128 rows (0 to 127, 128 to 255, ...) at most 8 rows name the same one
- route_weights: float32 [16384, 2], P(('sp', 'tp')), may hold values from 0.1 to 1
Outputs:
- result: bfloat16 [16384, 2048], P(('sp', 'tp'))
Inputs may be any that keep to these rules, and one draw needn't show every extreme that they name: `route_ids`: in each aligned block of 128 rows no expert is named by more than 8 rows, a bound that some block reaches.
All inputs are finite; a program needn't handle non-finite values.
Results may differ from a plain program's by a relative error of at most 0.015.
The roundings to bfloat16 on the way count: a program that leaves them out, or rounds other values in their place, can miss the bound.
Values may be sent and summed in bfloat16 or wider, within the bound.
A program may use at most 128 MiB of HBM per device.

v0:
```python
import math

import jax
import jax.numpy as jnp
from jax import lax
from jax.sharding import PartitionSpec as P

HA = 16
DA = 64
DB = 128
GRID_W = 128


eps = 1e-06
theta = 10000.0


def cut_along(value, dim, size):
    before, after = (value.shape[:dim], value.shape[dim + 1 :])
    return jnp.moveaxis(value.reshape(*before, size, -1, *after), dim, 0)


def summed_on_arrival(value, axis, dim):
    size = lax.axis_size(axis)
    blocks = lax.all_to_all(cut_along(value, dim, size), axis, 0, 0, tiled=True)
    return jnp.sum(blocks.astype(jnp.float32), axis=0)


def joined_along(blocks, dim):
    shape = list(blocks.shape[1:])
    shape[dim] *= blocks.shape[0]
    return jnp.moveaxis(blocks, 0, dim).reshape(shape)


def copy_for_each(value, axis):
    size = lax.axis_size(axis)
    return lax.all_to_all(
        jnp.broadcast_to(value[None], (size, *value.shape)), axis, 0, 0, tiled=True
    )


def gather_directly(value, axis, dim):
    return joined_along(copy_for_each(value, axis), dim)


def rotate_grid(normed, positions):
    count, heads, dim = normed.shape
    freqs = dim // 4
    inverse = theta ** (-jnp.arange(freqs, dtype=jnp.float32) / freqs)
    rows = (positions // GRID_W).astype(jnp.float32)
    cols = (positions % GRID_W).astype(jnp.float32)
    angles = jnp.stack([rows[:, None] * inverse, cols[:, None] * inverse], axis=1)
    cosine = jnp.cos(angles)[:, None]
    sine = jnp.sin(angles)[:, None]
    split = normed.reshape(count, heads, 2, 2, freqs)
    first = split[..., 0, :]
    second = split[..., 1, :]
    turned = jnp.stack([first * cosine - second * sine, second * cosine + first * sine], axis=-2)
    return turned.reshape(count, heads, dim)


def prepare(raw, gain, dim, positions):
    count = raw.shape[0]
    values = raw.astype(jnp.float32).reshape(count, -1, dim)
    scaled = values * lax.rsqrt(jnp.mean(values * values, axis=-1, keepdims=True) + eps) * gain
    return rotate_grid(scaled, positions).reshape(count, -1).astype(jnp.bfloat16)


def arrange(queries, kv_width, dim):
    rows = queries.shape[0]
    heads_kv = kv_width // dim
    shaped = queries.reshape(rows, heads_kv, -1, dim)
    groups = shaped.shape[2]
    start = (
        jnp.full((heads_kv, groups, rows), -1e30, jnp.float32),
        jnp.zeros((heads_kv, groups, rows), jnp.float32),
        jnp.zeros((heads_kv, groups, rows, dim), jnp.float32),
    )
    return (shaped, start)


def attend_block(state, queries, keys, values):
    peak, total, summed = state
    dim = queries.shape[-1]
    scores = jnp.einsum(
        "qhgd,khd->hgqk", queries, keys, preferred_element_type=jnp.float32
    ) * dim ** (-0.5)
    fresh = jnp.maximum(peak, jnp.max(scores, axis=-1))
    weights = jnp.exp(scores - fresh[..., None])
    shrink = jnp.exp(peak - fresh)
    total = total * shrink + jnp.sum(weights, axis=-1)
    summed = summed * shrink[..., None] + jnp.einsum(
        "hgqk,khd->hgqd", weights.astype(jnp.bfloat16), values, preferred_element_type=jnp.float32
    )
    return (fresh, total, summed)


def sweep(state, keys, values, queries):
    rows = keys.shape[0]
    size = math.gcd(rows, 2048)
    count = rows // size

    def step(carry, block):
        return (attend_block(carry, queries, block[0], block[1]), None)

    blocks = (
        keys.reshape(count, size, keys.shape[1], keys.shape[2]),
        values.reshape(count, size, values.shape[1], values.shape[2]),
    )
    state, _ = lax.scan(step, state, blocks)
    return state


def make_fold(shaped_n, shaped_b, state, pieces):
    keys_n, values_n, keys_b, values_b = pieces
    rows = keys_n.shape[0]
    first = sweep(state[0], keys_n.reshape(rows, -1, DA), values_n.reshape(rows, -1, DA), shaped_n)
    second = sweep(state[1], keys_b.reshape(rows, -1, DB), values_b.reshape(rows, -1, DB), shaped_b)
    return (first, second)


def finish(state):
    peak, total, summed = state
    heads_out = summed / total[..., None]
    rows = heads_out.shape[2]
    return jnp.transpose(heads_out, (2, 0, 1, 3)).reshape(rows, -1).astype(jnp.bfloat16)


def local(
    stream,
    query_narrow,
    key_narrow,
    value_narrow,
    query_broad,
    key_broad,
    value_broad,
    narrow_query_gain,
    narrow_key_gain,
    broad_query_gain,
    broad_key_gain,
    out_weight,
    norm_gain,
    gate_weight,
    up_weight,
    down_weight,
    route_ids,
    route_weights,
):
    count = query_narrow.shape[0]
    positions = lax.axis_index("sp") * count + jnp.arange(count, dtype=jnp.int32)
    queries_n = prepare(query_narrow, narrow_query_gain, DA, positions)
    keys_n = prepare(key_narrow, narrow_key_gain, DA, positions)
    queries_b = prepare(query_broad, broad_query_gain, DB, positions)
    keys_b = prepare(key_broad, broad_key_gain, DB, positions)
    shaped_n, start_n = arrange(queries_n, keys_n.shape[1], DA)
    shaped_b, start_b = arrange(queries_b, keys_b.shape[1], DB)
    state = make_fold(
        shaped_n,
        shaped_b,
        (start_n, start_b),
        (
            lax.all_gather(keys_n, "sp", axis=0, tiled=True),
            lax.all_gather(value_narrow, "sp", axis=0, tiled=True),
            lax.all_gather(keys_b, "sp", axis=0, tiled=True),
            lax.all_gather(value_broad, "sp", axis=0, tiled=True),
        ),
    )
    heads_n = finish(state[0])
    heads_b = finish(state[1])
    width = heads_n.shape[1]
    place = lax.axis_index("tp")
    local_weight = jnp.concatenate(
        [
            lax.dynamic_slice_in_dim(out_weight, place * width, width, 0),
            lax.dynamic_slice_in_dim(out_weight, HA * DA + place * width, width, 0),
        ],
        axis=0,
    )
    local_heads = jnp.concatenate([heads_n, heads_b], axis=1)
    picked = local_heads
    mixed = summed_on_arrival(
        jnp.dot(picked, local_weight, preferred_element_type=jnp.float32).astype(jnp.bfloat16),
        "tp",
        0,
    )
    wide = (stream.astype(jnp.float32) + mixed).astype(jnp.bfloat16).astype(jnp.float32)
    normed = (
        wide * lax.rsqrt(jnp.mean(wide * wide, axis=-1, keepdims=True) + eps) * norm_gain
    ).astype(jnp.bfloat16)
    tokens_here, topk = route_ids.shape
    width_model = normed.shape[1]
    experts = lax.axis_size("sp")
    capacity = (2 * tokens_here * topk + experts - 1) // experts
    flat = route_ids.reshape(-1)
    hits = (flat[:, None] == jnp.arange(experts, dtype=jnp.int32)[None, :]).astype(jnp.int32)
    ranks = jnp.sum((jnp.cumsum(hits, axis=0) - 1) * hits, axis=1)
    slots = flat * capacity + ranks
    table = (jnp.arange(experts * capacity, dtype=jnp.int32)[:, None] == slots[None, :]).astype(
        jnp.bfloat16
    )
    table = jnp.sum(table.reshape(experts * capacity, tokens_here, topk), axis=2)
    sent = jnp.dot(table, normed, preferred_element_type=jnp.float32).astype(jnp.bfloat16)
    sent = sent.reshape(experts, capacity, width_model)
    piece = gather_directly(
        lax.all_to_all(sent, "sp", split_axis=0, concat_axis=0, tiled=True), "tp", 0
    )
    rows = piece.reshape(-1, piece.shape[-1])
    gate = jnp.dot(rows, gate_weight[0], preferred_element_type=jnp.float32)
    upper = jnp.dot(rows, up_weight[0], preferred_element_type=jnp.float32)
    hidden = (jax.nn.silu(gate) * upper).astype(jnp.bfloat16)
    partial_out = jnp.dot(hidden, down_weight[0], preferred_element_type=jnp.float32).astype(
        jnp.bfloat16
    )
    terms = lax.optimization_barrier(partial_out).astype(jnp.float32).reshape(piece.shape)
    summed = summed_on_arrival(terms.astype(jnp.bfloat16), "tp", 0).astype(jnp.bfloat16)
    back = lax.all_to_all(summed, "sp", split_axis=0, concat_axis=0, tiled=True)
    picked = jnp.take(back.reshape(experts * capacity, width_model), slots, axis=0)
    picked = picked.astype(jnp.float32).reshape(tokens_here, topk, width_model)
    routed = jnp.sum(picked * route_weights[..., None], axis=1)
    return (wide + routed).astype(jnp.bfloat16)


def solution(mesh):
    return jax.shard_map(
        local,
        mesh=mesh,
        in_specs=(
            P(("sp", "tp"), None),
            P("sp", "tp"),
            P("sp", "tp"),
            P("sp", "tp"),
            P("sp", "tp"),
            P("sp", "tp"),
            P("sp", "tp"),
            P(),
            P(),
            P(),
            P(),
            P(),
            P(),
            P("sp", None, "tp"),
            P("sp", None, "tp"),
            P("sp", "tp", None),
            P(("sp", "tp"), None),
            P(("sp", "tp"), None),
        ),
        out_specs=P(("sp", "tp"), None),
        check_vma=False,
    )
```

profile of v0, /device:TPU:0, one launch (start us, length us, event | category | flops | bytes accessed | tf_op | source)
XLA Modules:
  0.0 630.0 jit_solution(12985772197260481180)
XLA Ops:
  25.9 53.0 %all-gather.5.cloned.1.call-done = bf16[16384,64]{0,1:T(8,128)(2,1)} async-done(((bf16[256,64]{0,1:T(8,128)(2,1)}), bf16[16384,64]{0,1:T(8,128)(2,1)}) %all-gather.5.cloned.1.call-update) | async-done | bytes 2097168 | tf_op jit(solution)/shard_map/all_gather | solution.py:162
  84.2 63.0 %all-gather.7.cloned.1.call-done = bf16[16384,64]{0,1:T(8,128)(2,1)} async-done(((bf16[256,64]{0,1:T(8,128)(2,1)}), bf16[16384,64]{0,1:T(8,128)(2,1)}) %all-gather.7.cloned.1.call-update) | async-done | bytes 2097168 | tf_op jit(solution)/shard_map/all_gather | solution.py:163
  152.5 220.2 %while.30 = (s32[]{:T(128)}, f32[1,8,256]{2,1,0:T(8,128)S(1)}, f32[1,8,256]{2,1,0:T(8,128)S(1)}, f32[1,8,256,64]{2,3,1,0:T(8,128)}, bf16[8,2048,1,64]{1,3,2,0:T(...) while((s32[]{:T(128)}, f32[1,8,256]{2,1,0:T(8,128)S(1)}, ...), condition=%wide.region_5.6_spmd.clone, body=%wide.region_2.5_spmd.clone.sunk | while | flops 1107701760 | bytes 52298852 | solution.py:110
  153.0 9.0 %bitcast_reduce_fusion.6 = (f32[8,256]{1,0:T(8,128)S(1)}, f32[2048,256,8]{1,0,2:T(8,128)}) fusion(bf16[256,1,8,64]{0,3,2,1:T(8,128)(2,1)S(1)} %get-tuple-element.395, bf16[8,2048,1,64]{1,3,2,0:T(8,128)(2,1)} %get-tuple-element.394, s32[]{:T(128)} %get-tuple-element.381), kind=kOutput, calls=%fused_computation.2.clone.1 | convolution fusion | flops 545257472 | bytes 17310208 | tf_op jit(solution)/shard_map/while/body/eval_jaxpr/qhgd,khd->hgqk/dot_general | solution.py:85
  162.0 9.6 %fusion.116 = f32[1,8,256,64]{2,3,1,0:T(8,128)} fusion(f32[2048,256,8]{1,0,2:T(8,128)} %get-tuple-element.332, f32[8,256]{1,0:T(8,128)S(1)} %bitcast.237, f32[1,8,256,64]{2,3,1,0:T(8,128)} %get-tuple-element.384, bf16[8,2048,1,64]{1,3,2,0:T(8,128)(2,1)} %get-tuple-element.396, s32[]{:T(128)} %get-tuple-element.381, ...), kind=kOutput, calls=%fused_computation.9.clone.1 | convolution fusion | flops 549847040 | bytes 18104832 | tf_op jit(solution)/shard_map/while/body/eval_jaxpr/hgqk,khd->hgqd/dot_general | solution.py:92
  180.3 9.0 %bitcast_reduce_fusion.6 = (f32[8,256]{1,0:T(8,128)S(1)}, f32[2048,256,8]{1,0,2:T(8,128)}) fusion(bf16[256,1,8,64]{0,3,2,1:T(8,128)(2,1)S(1)} %get-tuple-element.395, bf16[8,2048,1,64]{1,3,2,0:T(8,128)(2,1)} %get-tuple-element.394, s32[]{:T(128)} %get-tuple-element.381), kind=kOutput, calls=%fused_computation.2.clone.1 | convolution fusion | flops 545257472 | bytes 17310208 | tf_op jit(solution)/shard_map/while/body/eval_jaxpr/qhgd,khd->hgqk/dot_general | solution.py:85
  189.3 9.7 %fusion.116 = f32[1,8,256,64]{2,3,1,0:T(8,128)} fusion(f32[2048,256,8]{1,0,2:T(8,128)} %get-tuple-element.332, f32[8,256]{1,0:T(8,128)S(1)} %bitcast.237, f32[1,8,256,64]{2,3,1,0:T(8,128)} %get-tuple-element.384, bf16[8,2048,1,64]{1,3,2,0:T(8,128)(2,1)} %get-tuple-element.396, s32[]{:T(128)} %get-tuple-element.381, ...), kind=kOutput, calls=%fused_computation.9.clone.1 | convolution fusion | flops 549847040 | bytes 18104832 | tf_op jit(solution)/shard_map/while/body/eval_jaxpr/hgqk,khd->hgqd/dot_general | solution.py:92
  208.0 9.0 %bitcast_reduce_fusion.6 = (f32[8,256]{1,0:T(8,128)S(1)}, f32[2048,256,8]{1,0,2:T(8,128)}) fusion(bf16[256,1,8,64]{0,3,2,1:T(8,128)(2,1)S(1)} %get-tuple-element.395, bf16[8,2048,1,64]{1,3,2,0:T(8,128)(2,1)} %get-tuple-element.394, s32[]{:T(128)} %get-tuple-element.381), kind=kOutput, calls=%fused_computation.2.clone.1 | convolution fusion | flops 545257472 | bytes 17310208 | tf_op jit(solution)/shard_map/while/body/eval_jaxpr/qhgd,khd->hgqk/dot_general | solution.py:85
  217.0 10.0 %fusion.116 = f32[1,8,256,64]{2,3,1,0:T(8,128)} fusion(f32[2048,256,8]{1,0,2:T(8,128)} %get-tuple-element.332, f32[8,256]{1,0:T(8,128)S(1)} %bitcast.237, f32[1,8,256,64]{2,3,1,0:T(8,128)} %get-tuple-element.384, bf16[8,2048,1,64]{1,3,2,0:T(8,128)(2,1)} %get-tuple-element.396, s32[]{:T(128)} %get-tuple-element.381, ...), kind=kOutput, calls=%fused_computation.9.clone.1 | convolution fusion | flops 549847040 | bytes 18104832 | tf_op jit(solution)/shard_map/while/body/eval_jaxpr/hgqk,khd->hgqd/dot_general | solution.py:92
  235.6 9.0 %bitcast_reduce_fusion.6 = (f32[8,256]{1,0:T(8,128)S(1)}, f32[2048,256,8]{1,0,2:T(8,128)}) fusion(bf16[256,1,8,64]{0,3,2,1:T(8,128)(2,1)S(1)} %get-tuple-element.395, bf16[8,2048,1,64]{1,3,2,0:T(8,128)(2,1)} %get-tuple-element.394, s32[]{:T(128)} %get-tuple-element.381), kind=kOutput, calls=%fused_computation.2.clone.1 | convolution fusion | flops 545257472 | bytes 17310208 | tf_op jit(solution)/shard_map/while/body/eval_jaxpr/qhgd,khd->hgqk/dot_general | solution.py:85
  244.7 9.7 %fusion.116 = f32[1,8,256,64]{2,3,1,0:T(8,128)} fusion(f32[2048,256,8]{1,0,2:T(8,128)} %get-tuple-element.332, f32[8,256]{1,0:T(8,128)S(1)} %bitcast.237, f32[1,8,256,64]{2,3,1,0:T(8,128)} %get-tuple-element.384, bf16[8,2048,1,64]{1,3,2,0:T(8,128)(2,1)} %get-tuple-element.396, s32[]{:T(128)} %get-tuple-element.381, ...), kind=kOutput, calls=%fused_computation.9.clone.1 | convolution fusion | flops 549847040 | bytes 18104832 | tf_op jit(solution)/shard_map/while/body/eval_jaxpr/hgqk,khd->hgqd/dot_general | solution.py:92
  263.0 9.0 %bitcast_reduce_fusion.6 = (f32[8,256]{1,0:T(8,128)S(1)}, f32[2048,256,8]{1,0,2:T(8,128)}) fusion(bf16[256,1,8,64]{0,3,2,1:T(8,128)(2,1)S(1)} %get-tuple-element.395, bf16[8,2048,1,64]{1,3,2,0:T(8,128)(2,1)} %get-tuple-element.394, s32[]{:T(128)} %get-tuple-element.381), kind=kOutput, calls=%fused_computation.2.clone.1 | convolution fusion | flops 545257472 | bytes 17310208 | tf_op jit(solution)/shard_map/while/body/eval_jaxpr/qhgd,khd->hgqk/dot_general | solution.py:85
  272.1 9.7 %fusion.116 = f32[1,8,256,64]{2,3,1,0:T(8,128)} fusion(f32[2048,256,8]{1,0,2:T(8,128)} %get-tuple-element.332, f32[8,256]{1,0:T(8,128)S(1)} %bitcast.237, f32[1,8,256,64]{2,3,1,0:T(8,128)} %get-tuple-element.384, bf16[8,2048,1,64]{1,3,2,0:T(8,128)(2,1)} %get-tuple-element.396, s32[]{:T(128)} %get-tuple-element.381, ...), kind=kOutput, calls=%fused_computation.9.clone.1 | convolution fusion | flops 549847040 | bytes 18104832 | tf_op jit(solution)/shard_map/while/body/eval_jaxpr/hgqk,khd->hgqd/dot_general | solution.py:92
  290.8 9.0 %bitcast_reduce_fusion.6 = (f32[8,256]{1,0:T(8,128)S(1)}, f32[2048,256,8]{1,0,2:T(8,128)}) fusion(bf16[256,1,8,64]{0,3,2,1:T(8,128)(2,1)S(1)} %get-tuple-element.395, bf16[8,2048,1,64]{1,3,2,0:T(8,128)(2,1)} %get-tuple-element.394, s32[]{:T(128)} %get-tuple-element.381), kind=kOutput, calls=%fused_computation.2.clone.1 | convolution fusion | flops 545257472 | bytes 17310208 | tf_op jit(solution)/shard_map/while/body/eval_jaxpr/qhgd,khd->hgqk/dot_general | solution.py:85
  299.8 9.7 %fusion.116 = f32[1,8,256,64]{2,3,1,0:T(8,128)} fusion(f32[2048,256,8]{1,0,2:T(8,128)} %get-tuple-element.332, f32[8,256]{1,0:T(8,128)S(1)} %bitcast.237, f32[1,8,256,64]{2,3,1,0:T(8,128)} %get-tuple-element.384, bf16[8,2048,1,64]{1,3,2,0:T(8,128)(2,1)} %get-tuple-element.396, s32[]{:T(128)} %get-tuple-element.381, ...), kind=kOutput, calls=%fused_computation.9.clone.1 | convolution fusion | flops 549847040 | bytes 18104832 | tf_op jit(solution)/shard_map/while/body/eval_jaxpr/hgqk,khd->hgqd/dot_general | solution.py:92
  318.1 9.0 %bitcast_reduce_fusion.6 = (f32[8,256]{1,0:T(8,128)S(1)}, f32[2048,256,8]{1,0,2:T(8,128)}) fusion(bf16[256,1,8,64]{0,3,2,1:T(8,128)(2,1)S(1)} %get-tuple-element.395, bf16[8,2048,1,64]{1,3,2,0:T(8,128)(2,1)} %get-tuple-element.394, s32[]{:T(128)} %get-tuple-element.381), kind=kOutput, calls=%fused_computation.2.clone.1 | convolution fusion | flops 545257472 | bytes 17310208 | tf_op jit(solution)/shard_map/while/body/eval_jaxpr/qhgd,khd->hgqk/dot_general | solution.py:85
  327.1 9.7 %fusion.116 = f32[1,8,256,64]{2,3,1,0:T(8,128)} fusion(f32[2048,256,8]{1,0,2:T(8,128)} %get-tuple-element.332, f32[8,256]{1,0:T(8,128)S(1)} %bitcast.237, f32[1,8,256,64]{2,3,1,0:T(8,128)} %get-tuple-element.384, bf16[8,2048,1,64]{1,3,2,0:T(8,128)(2,1)} %get-tuple-element.396, s32[]{:T(128)} %get-tuple-element.381, ...), kind=kOutput, calls=%fused_computation.9.clone.1 | convolution fusion | flops 549847040 | bytes 18104832 | tf_op jit(solution)/shard_map/while/body/eval_jaxpr/hgqk,khd->hgqd/dot_general | solution.py:92
  345.4 9.0 %bitcast_reduce_fusion.6 = (f32[8,256]{1,0:T(8,128)S(1)}, f32[2048,256,8]{1,0,2:T(8,128)}) fusion(bf16[256,1,8,64]{0,3,2,1:T(8,128)(2,1)S(1)} %get-tuple-element.395, bf16[8,2048,1,64]{1,3,2,0:T(8,128)(2,1)} %get-tuple-element.394, s32[]{:T(128)} %get-tuple-element.381), kind=kOutput, calls=%fused_computation.2.clone.1 | convolution fusion | flops 545257472 | bytes 17310208 | tf_op jit(solution)/shard_map/while/body/eval_jaxpr/qhgd,khd->hgqk/dot_general | solution.py:85
  354.4 9.7 %fusion.116 = f32[1,8,256,64]{2,3,1,0:T(8,128)} fusion(f32[2048,256,8]{1,0,2:T(8,128)} %get-tuple-element.332, f32[8,256]{1,0:T(8,128)S(1)} %bitcast.237, f32[1,8,256,64]{2,3,1,0:T(8,128)} %get-tuple-element.384, bf16[8,2048,1,64]{1,3,2,0:T(8,128)(2,1)} %get-tuple-element.396, s32[]{:T(128)} %get-tuple-element.381, ...), kind=kOutput, calls=%fused_computation.9.clone.1 | convolution fusion | flops 549847040 | bytes 18104832 | tf_op jit(solution)/shard_map/while/body/eval_jaxpr/hgqk,khd->hgqd/dot_general | solution.py:92
  380.8 103.1 %while.31 = (s32[]{:T(128)}, f32[1,4,256]{2,1,0:T(4,128)S(1)}, f32[1,4,256]{2,1,0:T(4,128)S(1)}, f32[1,4,256,128]{3,2,1,0:T(8,128)S(1)}, bf16[8,2048,1,128]{3,1,...) while((s32[]{:T(128)}, f32[1,4,256]{2,1,0:T(4,128)S(1)}, ...), condition=%wide.region_11.12_spmd.clone, body=%wide.region_8.11_spmd.clone.sunk | while | flops 1090918400 | bytes 61146240 | solution.py:110
  493.7 38.3 %all_to_all.26 = bf16[64,8,2048]{2,1,0:T(8,128)(2,1)S(1)} all-to-all(bf16[64,8,2048]{2,1,0:T(8,128)(2,1)S(1)} %fusion.48), channel_id=1, replica_groups=mesh['sp'=64,'tp'=2] {'sp'}, dimensions={0} | all-to-all | bytes 4194304 | tf_op jit(solution)/shard_map/all_to_all | solution.py:205
  545.7 10.1 %convolution_convert_fusion = bf16[1024,2048]{1,0:T(8,128)(2,1)} fusion(bf16[1,512,2048]{2,1,0:T(8,128)(2,1)S(1)} %copy-done, f32[1024,512]{1,0:T(8,128)} %fusion.53, bf16[1024,2048]{1,0:T(8,128)(2,1)} %bitcast.240, bf16[1,2048,512]{2,1,0:T(8,128)(2,1)} %param.35), kind=kOutput, calls=%fused_computation.53 | convolution fusion | flops 4300210176 | bytes 14680064 | tf_op jit(solution)/shard_map/dot_general | solution.py:211
  555.7 11.9 %all_to_all.28 = bf16[2,64,8,2048]{3,2,1,0:T(8,128)(2,1)} all-to-all(bf16[2,64,8,2048]{3,2,1,0:T(8,128)(2,1)} %bitcast.241), channel_id=1, replica_groups=mesh['sp'=64,'tp'=2] {'tp'}, dimensions={0} | all-to-all | bytes 8388608 | tf_op jit(solution)/shard_map/all_to_all | solution.py:25
  579.4 29.6 %all-to-all-done.4 = bf16[64,8,2048]{2,1,0:T(8,128)(2,1)} async-done(((bf16[64,8,2048]{2,1,0:T(8,128)(2,1)}), bf16[64,8,2048]{2,1,0:T(8,128)(2,1)}, u32[]{:S(2)}, u32[]{:S(2)}) %all-to-all-start.4) | async-done | bytes 2097184 | tf_op jit(solution)/shard_map/all_to_all | solution.py:216
  (211 shorter events, 259.2 us)
Async XLA Ops:
  6.5 539.1 %copy-start = (bf16[1,512,2048]{2,1,0:T(8,128)(2,1)S(1)}, bf16[1,512,2048]{2,1,0:T(8,128)(2,1)}, u32[]{:S(2)}) copy-start(bf16[1,512,2048]{2,1,0:T(8,128)(2,1)} %param.37) | copy-start | bytes 6291460
  6.5 13.6 %copy-start.6 = (s32[128,2]{0,1:T(2,128)S(1)}, s32[128,2]{0,1:T(2,128)}, u32[]{:S(2)}) copy-start(s32[128,2]{0,1:T(2,128)} %param.38) | copy-start | bytes 3076
  6.5 72.4 %all-gather.5.cloned.1.call-start = ((), (), s32[]{:S(2)}) async-start(), calls=%async_computation.5 | async-start | bytes 2129920 | tf_op jit(solution)/shard_map/all_gather | solution.py:162
  9.2 138.0 %all-gather.7.cloned.1.call-start = ((), (), s32[]{:S(2)}) async-start(), calls=%async_computation.6 | async-start | bytes 2129920 | tf_op jit(solution)/shard_map/all_gather | solution.py:163
  9.9 364.5 %all-gather.9.cloned.1.call-start = ((), (), s32[]{:S(2)}) async-start(), calls=%async_computation.7 | async-start | bytes 4259840 | tf_op jit(solution)/shard_map/all_gather | solution.py:164
  12.7 368.1 %all-gather.11.cloned.1.call-start = ((), (), s32[]{:S(2)}) async-start(), calls=%async_computation.8 | async-start | bytes 4259840 | tf_op jit(solution)/shard_map/all_gather | solution.py:165
  19.9 0.8 copy-start.4
  386.5 5.9 copy-start.1
  399.4 5.9 copy-start.1
  412.2 5.9 copy-start.1
  425.1 5.9 copy-start.1
  437.9 5.9 copy-start.1
  450.8 5.9 copy-start.1
  463.7 5.9 copy-start.1
  476.5 5.9 copy-start.1
  487.7 4.9 copy-start.3
  487.7 5.2 copy-start.8
  532.5 9.4 %copy-start.11 = (bf16[1,2048,512]{2,1,0:T(8,128)(2,1)S(1)}, bf16[1,2048,512]{2,1,0:T(8,128)(2,1)}, u32[]{:S(2)}) copy-start(bf16[1,2048,512]{2,1,0:T(8,128)(2,1)} %param.36) | copy-start | bytes 6291460
  540.0 2.0 copy-start.2
  567.6 11.3 %copy-start.7 = (s32[128,2]{0,1:T(2,128)S(1)}, s32[128,2]{0,1:T(2,128)}, u32[]{:S(2)}) copy-start(s32[128,2]{0,1:T(2,128)} %param.38) | copy-start | bytes 3076
  567.6 11.6 %copy-start.9 = (pred[128,2]{0,1:T(4,128)(4,1)S(1)}, pred[128,2]{0,1:T(4,128)(4,1)}, u32[]{:S(2)}) copy-start(pred[128,2]{0,1:T(4,128)(4,1)} %get-tuple-element.207) | copy-start | bytes 772
  567.6 11.7 %copy-start.10 = (f32[128,2]{0,1:T(2,128)S(1)}, f32[128,2]{0,1:T(2,128)}, u32[]{:S(2)}) copy-start(f32[128,2]{0,1:T(2,128)} %param.39) | copy-start | bytes 3076
  567.6 11.8 %copy-start.5 = (s32[256]{0:T(256)S(1)}, s32[256]{0:T(256)}, u32[]{:S(2)}) copy-start(s32[256]{0:T(256)} %copy-done.4) | copy-start | bytes 3076
  572.7 36.4 %all-to-all-start.4 = ((bf16[64,8,2048]{2,1,0:T(8,128)(2,1)}), bf16[64,8,2048]{2,1,0:T(8,128)(2,1)}, u32[]{:S(2)}, u32[]{:S(2)}) async-start(bf16[64,8,2048]{2,1,0:T(8,128)(2,1)} %reduce_sum.131), calls=%async_computation.4 | async-start | bytes 4194304 | tf_op jit(solution)/shard_map/all_to_all | solution.py:216
Sparse Core Ops, SparseCore 0:
  10.0 68.8 all-gather.4
  81.6 65.5 all-gather.6
  149.9 74.0 all-gather.8
  226.7 69.3 all-gather.10
where the time goes:
time: 638 us; the launch traced here: 630 us
  matrix products  254 us (40%)
  waiting for transfers between devices  147 us (23%)
  other arithmetic  101 us (16%)
  blocking collectives  62.3 us (10%)
  local copies, waits for them, and re-layouts  44.2 us (7%)
  between operations  13.8 us (2%)
    dot_general x16, matrix products, attend_block(): jnp.einsum('hgqk,khd->hgqd', weights.astype(jnp.bfloat16), values, prefer...  120 us
    dot_general x16, matrix products, attend_block(): jnp.einsum('qhgd,khd->hgqk', queries, keys, preferred_element_type=jnp.fl...  116 us
    reduce_sum x16, other arithmetic, attend_block(): total = total * shrink + jnp.sum(weights, axis=-1)  80.2 us
    all_gather x1, waiting for transfers between devices, local(): lax.all_gather(value_narrow, 'sp', axis=0, tiled=True)  63 us
    all_gather x1, waiting for transfers between devices, local(): lax.all_gather(keys_n, 'sp', axis=0, tiled=True)  53 us
    all_to_all x1, blocking collectives, local(): lax.all_to_all(sent, 'sp', split_axis=0, concat_axis=0, tiled=True)  38.3 us
    all_to_all x1, waiting for transfers between devices, local(): back = lax.all_to_all(summed, 'sp', split_axis=0, concat_axis=0, tiled=True)  29.6 us
    unnamed x33, local copies, waits for them, and re-layouts  23.1 us
  transfers between devices with their start and end apart: 5, of which 3 were waited for; matrix products, arithmetic and copies ran while one was open for 40% of the time, Pallas kernels for 0%

commit v1 on v0

v1 whole, which is shorter than its diff:
```python
import functools
import math

import jax
import jax.numpy as jnp
import numpy as np
from jax import lax
from jax.experimental import pallas as pl
from jax.experimental.pallas import tpu as pltpu
from jax.sharding import PartitionSpec as P

F32 = jnp.float32
BF = jnp.bfloat16
MESH = pl.DeviceIdType.MESH
eps = 1e-06
theta = 10000.0
LOG2E = math.log2(math.e)
NB = 4
ORDERS = ((2, 1, 0), (1, 0, 2), (0, 2, 1))
OFFSETS = (0, -1, 1, 2)


def sem_index(piece, phase, item, way):
    base = (0, 4, 20)[phase]
    return piece * 36 + base + item * 4 + way


def inverse_table():
    parts = []
    for dim in (64, 128):
        freqs = dim // 4
        inv = np.float32(theta) ** (-np.arange(freqs, dtype=np.float32) / np.float32(freqs))
        parts.append(np.broadcast_to(inv.astype(np.float32)[:, None], (freqs, 256)))
    return np.concatenate(parts, axis=0)


def rotate(x, cosr, sinr, cosc, sinc):
    f = x.shape[0] // 4
    a, b, c, d = x[:f], x[f : 2 * f], x[2 * f : 3 * f], x[3 * f :]
    return jnp.concatenate(
        [a * cosr - b * sinr, b * cosr + a * sinr, c * cosc - d * sinc, d * cosc + c * sinc], axis=0
    )


def normed_rows(x, gain):
    mean = jnp.mean(x * x, axis=0, keepdims=True)
    return x * lax.rsqrt(mean + eps) * gain


def gain_column(g_ref):
    g = g_ref[...]
    if g.shape[1] == 64:
        g = jnp.concatenate([g, g], axis=1)
    col = jnp.broadcast_to(g, (128, 128)).T
    return jnp.concatenate([col, col], axis=1)


def attention_kernel(
    qn_ref, kn_ref, vn_ref, qb_ref, kb_ref, vb_ref, gqn_ref, gkn_ref, gqb_ref, gkb_ref, inv_ref,
    out_ref,
    kv, qna, qnb, qbt, s_scr, st_m, st_l, on, ob, heads, send_sem, recv_sem, tp_send, tp_recv,
):
    sp = lax.axis_index("sp")
    tp = lax.axis_index("tp")
    me = (sp // 16, (sp // 4) % 4, sp % 4)

    def neighbour(dim, step):
        at = list(me)
        at[dim] = (at[dim] + step + 4) % 4
        return (at[0] * 4 + at[1]) * 4 + at[2]

    barrier = pltpu.get_barrier_semaphore()
    for dim in range(3):
        for step in (1, -1):
            pl.semaphore_signal(barrier, inc=1, device_id=(neighbour(dim, step), tp), device_id_type=MESH)
    pl.semaphore_signal(barrier, inc=1, device_id=(sp, 1 - tp), device_id_type=MESH)

    lane = lax.broadcasted_iota(jnp.int32, (8, 256), 1)
    rows_of = ((lane // 128) + sp * 2).astype(F32)
    cols_of = (lane % 128).astype(F32)

    def tables(first, freqs):
        inv = inv_ref[first : first + freqs, :]
        r = jnp.concatenate([rows_of] * (freqs // 8), axis=0) * inv
        c = jnp.concatenate([cols_of] * (freqs // 8), axis=0) * inv
        return jnp.cos(r), jnp.sin(r), jnp.cos(c), jnp.sin(c)

    tab_n = tables(0, 16)
    tab_b = tables(16, 32)

    kvn = jnp.concatenate([kn_ref[...].astype(F32), vn_ref[...].astype(F32)], axis=1).T
    kt = rotate(normed_rows(kvn[:64], gain_column(gkn_ref)[:64]), *tab_n)
    vt = kvn[64:]
    here = kv.at[me[0], me[1], me[2]]
    here[0:128, :] = jnp.concatenate([kt[:, :128], kt[:, 128:]], axis=0).T.astype(BF)
    here[128:256, :] = jnp.concatenate([vt[:, :128], vt[:, 128:]], axis=0).astype(BF)
    kbt = rotate(normed_rows(kb_ref[...].astype(F32).T, gain_column(gkb_ref)), *tab_b)
    here[256:512, :] = kbt.T.astype(BF)
    vbt = vb_ref[...].astype(F32).T
    here[512:768, :] = jnp.concatenate([vbt[:, :128], vbt[:, 128:]], axis=0).astype(BF)

    pl.semaphore_wait(barrier, 7)

    def part(piece, phase, item, way, mine):
        order = ORDERS[piece]
        at = [me[0], me[1], me[2]]
        rows = pl.ds(piece * 256, 256)
        if phase == 1:
            at[order[0]] = (me[order[0]] + OFFSETS[item] + 4) % 4
        if phase == 2:
            at[order[1]] = (me[order[1]] + OFFSETS[item] + 4) % 4
            at[order[0]] = pl.ds(0, 4)
        back = {0: 0, 1: 0, 2: -1, 3: 1}[way] if mine else {0: -1, 1: 1, 2: -2, 3: 2}[way]
        at[order[phase]] = (me[order[phase]] + back + 4) % 4
        if way >= 2:
            if phase == 2:
                at[order[0]] = pl.ds((way - 2) * 2, 2)
            else:
                rows = pl.ds(piece * 256 + (way - 2) * 128, 128)
        return kv.at[at[0], at[1], at[2], rows]

    def copy_of(piece, phase, item, way, mine):
        ref = part(piece, phase, item, way, mine)
        index = sem_index(piece, phase, item, way)
        to = neighbour(ORDERS[piece][phase], (1, -1, 1, -1)[way])
        return pltpu.make_async_remote_copy(
            src_ref=ref, dst_ref=ref, send_sem=send_sem.at[index], recv_sem=recv_sem.at[index],
            device_id=(to, tp), device_id_type=MESH,
        )

    def send(piece, phase, item):
        copy_of(piece, phase, item, 0, True).start()
        copy_of(piece, phase, item, 1, True).start()

    def arrive(piece, phase, item, way):
        copy_of(piece, phase, item, way, False).wait_recv()
        if way < 2:
            copy_of(piece, phase, item, way + 2, True).start()

    pieces = range(3)
    for p in pieces:
        send(p, 0, 0)
    for p in pieces:
        send(p, 1, 0)

    zero = jnp.zeros((64, 256), BF)
    gq = gain_column(gqn_ref)[:64]
    for pair in range(4):
        qt = qn_ref[:, pair * 128 : pair * 128 + 128].astype(F32).T
        for half in range(2):
            h = pair * 2 + half
            q = rotate(normed_rows(qt[half * 64 : half * 64 + 64], gq), *tab_n).astype(BF)
            q = q.astype(F32) * (64 ** -0.5 * LOG2E)
            hi = q.astype(BF)
            lo = (q - hi.astype(F32)).astype(BF)
            qna[h] = jnp.concatenate([hi, zero, lo, zero], axis=0)
            qnb[h] = jnp.concatenate([zero, hi, zero, lo], axis=0)
    gq = gain_column(gqb_ref)
    for h in range(4):
        qt = qb_ref[:, h * 128 : h * 128 + 128].astype(F32).T
        q = rotate(normed_rows(qt, gq), *tab_b).astype(BF)
        q = q.astype(F32) * (128 ** -0.5 * LOG2E)
        hi = q.astype(BF)
        lo = (q - hi.astype(F32)).astype(BF)
        qbt[h] = jnp.concatenate([hi, lo], axis=0)

    st_m[...] = jnp.full(st_m.shape, -1e30, F32)
    st_l[...] = jnp.zeros(st_l.shape, F32)
    on[...] = jnp.zeros(on.shape, F32)
    ob[...] = jnp.zeros(ob.shape, F32)

    def qk(t, zz, yy, slot):
        mx = None
        for u in range(NB):
            if t < 8:
                k = kv[zz, yy, u, 0:128, :]
                k2 = jnp.concatenate([k, k], axis=1)
                sa = jnp.dot(k2, qna[t], preferred_element_type=F32)
                sb = jnp.dot(k2, qnb[t], preferred_element_type=F32)
                s = jnp.concatenate([sa, sb], axis=0)
            else:
                k = kv[zz, yy, u, 256:512, :]
                k2 = jnp.concatenate([k, k], axis=1)
                s = jnp.dot(k2, qbt[t - 8], preferred_element_type=F32)
            s_scr[slot, pl.ds(u * 256, 256), :] = s
            r = jnp.max(s.reshape(32, 8, 256), axis=0)
            mx = r if mx is None else jnp.maximum(mx, r)
        return mx

    def pv(t, zz, yy, slot, mx):
        m_old = st_m[t]
        mm = jnp.max(jnp.maximum(mx, m_old), axis=0, keepdims=True)
        alpha = jnp.exp2(m_old[0:1] - mm)
        ps, vs, ls = [], [], None
        for u in range(NB):
            p = jnp.exp2(s_scr[slot, pl.ds(u * 256, 256), :] - mm)
            l = jnp.sum(p.reshape(32, 8, 256), axis=0)
            ls = l if ls is None else ls + l
            ps.append(p.astype(BF))
            if t < 8:
                vs.append(kv[zz, yy, u, 128:192, :])
                vs.append(kv[zz, yy, u, 192:256, :])
            else:
                vs.append(kv[zz, yy, u, 512:640, :])
                vs.append(kv[zz, yy, u, 640:768, :])
        o = jnp.dot(jnp.concatenate(vs, axis=1), jnp.concatenate(ps, axis=0), preferred_element_type=F32)
        st_m[t] = jnp.broadcast_to(mm, (8, 256))
        st_l[t] = st_l[t] * alpha + ls
        if t < 8:
            on[t] = on[t] * alpha + o
        else:
            ob[t - 8] = ob[t - 8] * alpha + o

    def block(first, last, zz, yy):
        mx = qk(first, zz, yy, 0)
        for t in range(first, last):
            slot = (t - first) % 2
            nx = qk(t + 1, zz, yy, 1 - slot) if t + 1 < last else None
            pv(t, zz, yy, slot, mx)
            mx = nx

    def opening():
        for p in pieces:
            arrive(p, 0, 0, 0)
            arrive(p, 0, 0, 1)
            send(p, 1, 1)
            send(p, 1, 2)
        for p in pieces:
            arrive(p, 1, 0, 0)
            arrive(p, 1, 0, 1)
        for p in pieces:
            arrive(p, 0, 0, 2)
            arrive(p, 0, 0, 3)
            send(p, 1, 3)
            send(p, 2, 0)

    def second():
        for item in (1, 2):
            for p in pieces:
                arrive(p, 1, item, 0)
                arrive(p, 1, item, 1)
        for p in pieces:
            arrive(p, 1, 3, 0)
            arrive(p, 1, 3, 1)
            send(p, 2, 1)
            send(p, 2, 2)

    def third():
        for p in pieces:
            for item in range(4):
                arrive(p, 1, item, 2)
                arrive(p, 1, item, 3)
            send(p, 2, 3)

    def sides(item):
        for p in pieces:
            arrive(p, 2, item, 0)
            arrive(p, 2, item, 1)

    def far(item):
        for p in pieces:
            arrive(p, 2, item, 2)
            arrive(p, 2, item, 3)

    events = {1: second, 3: third}
    for k in range(4):
        events[4 + 2 * k] = functools.partial(sides, k)
        events[12 + k] = functools.partial(far, k)

    def chunk_offset(c):
        return (c % 2) * 3 * (1 - c // 2) + (c // 2) * (1 + c % 2)

    def narrow_round(i, _):
        for at, event in events.items():
            pl.when(i == at)(event)
        early = 1 - jnp.minimum(i // 4, 1)
        late = i // 12
        middle = 1 - early - late
        k = i - 4
        c = early * i + middle * (k // 2) + late * (i - 12)
        zo = middle * (3 - 2 * (k % 2)) + late * 2
        zz = (me[0] + zo) % 4
        yy = (me[1] + chunk_offset(c)) % 4
        block(0, 8, zz, yy)
        return 0

    def broad_round(i, _):
        block(8, 12, i // 4, i % 4)
        return 0

    opening()
    lax.fori_loop(0, 16, narrow_round, 0)
    lax.fori_loop(0, 16, broad_round, 0)

    for pair in range(4):
        cols = []
        for t in (2 * pair, 2 * pair + 1):
            cols.append(on[t] / jnp.sum(st_l[t], axis=0, keepdims=True))
        heads[:, pair * 128 : pair * 128 + 128] = jnp.concatenate(cols, axis=0).T.astype(BF)
    for t in range(4):
        o = ob[t] / jnp.sum(st_l[8 + t], axis=0, keepdims=True)
        heads[:, 512 + t * 128 : 640 + t * 128] = o.T.astype(BF)

    mine = pl.ds(pl.multiple_of(tp * 128, 128), 128)
    other = pl.ds(pl.multiple_of((1 - tp) * 128, 128), 128)
    swaps = []
    for g in range(2):
        place = pl.ds(pl.multiple_of(g * 1024 + tp * 512, 128), 512)
        swap = pltpu.make_async_remote_copy(
            src_ref=heads.at[other, pl.ds(g * 512, 512)], dst_ref=out_ref.at[:, place],
            send_sem=tp_send.at[g], recv_sem=tp_recv.at[g], device_id=(sp, 1 - tp), device_id_type=MESH,
        )
        swap.start()
        swaps.append(swap)
        out_ref[:, place] = heads[mine, pl.ds(g * 512, 512)]
    for p in pieces:
        for phase in range(3):
            for item in range(1 if phase == 0 else 4):
                for way in range(4):
                    copy_of(p, phase, item, way, True).wait_send()
    for g in range(2):
        place = pl.ds(pl.multiple_of(g * 1024 + (1 - tp) * 512, 128), 512)
        pltpu.make_async_remote_copy(
            src_ref=heads.at[other, pl.ds(g * 512, 512)], dst_ref=out_ref.at[:, place],
            send_sem=tp_send.at[g], recv_sem=tp_recv.at[g], device_id=(sp, 1 - tp), device_id_type=MESH,
        ).wait_recv()
        swaps[g].wait_send()


def attention(qn, kn, vn, qb, kb, vb, gqn, gkn, gqb, gkb):
    inv = jnp.asarray(inverse_table())
    vm = pl.BlockSpec(memory_space=pltpu.VMEM)
    return pl.pallas_call(
        attention_kernel,
        out_shape=jax.ShapeDtypeStruct((128, 2048), BF),
        in_specs=[vm] * 11,
        out_specs=vm,
        scratch_shapes=[
            pltpu.VMEM((4, 4, 4, 768, 128), BF),
            pltpu.VMEM((8, 256, 256), BF),
            pltpu.VMEM((8, 256, 256), BF),
            pltpu.VMEM((4, 256, 256), BF),
            pltpu.VMEM((2, NB * 256, 256), F32),
            pltpu.VMEM((12, 8, 256), F32),
            pltpu.VMEM((12, 8, 256), F32),
            pltpu.VMEM((8, 64, 256), F32),
            pltpu.VMEM((4, 128, 256), F32),
            pltpu.VMEM((256, 1024), BF),
            pltpu.SemaphoreType.DMA((108,)),
            pltpu.SemaphoreType.DMA((108,)),
            pltpu.SemaphoreType.DMA((2,)),
            pltpu.SemaphoreType.DMA((2,)),
        ],
        compiler_params=pltpu.CompilerParams(
            collective_id=0, has_side_effects=True, vmem_limit_bytes=60 * 1024 * 1024
        ),
        name="attention",
    )(
        qn, kn, vn, qb, kb, vb,
        gqn.reshape(1, -1), gkn.reshape(1, -1), gqb.reshape(1, -1), gkb.reshape(1, -1), inv,
    )


def cut_along(value, dim, size):
    before, after = (value.shape[:dim], value.shape[dim + 1 :])
    return jnp.moveaxis(value.reshape(*before, size, -1, *after), dim, 0)


def summed_on_arrival(value, axis, dim):
    size = lax.axis_size(axis)
    blocks = lax.all_to_all(cut_along(value, dim, size), axis, 0, 0, tiled=True)
    return jnp.sum(blocks.astype(jnp.float32), axis=0)


def joined_along(blocks, dim):
    shape = list(blocks.shape[1:])
    shape[dim] *= blocks.shape[0]
    return jnp.moveaxis(blocks, 0, dim).reshape(shape)


def copy_for_each(value, axis):
    size = lax.axis_size(axis)
    return lax.all_to_all(
        jnp.broadcast_to(value[None], (size, *value.shape)), axis, 0, 0, tiled=True
    )


def gather_directly(value, axis, dim):
    return joined_along(copy_for_each(value, axis), dim)


def local(
    stream,
    query_narrow,
    key_narrow,
    value_narrow,
    query_broad,
    key_broad,
    value_broad,
    narrow_query_gain,
    narrow_key_gain,
    broad_query_gain,
    broad_key_gain,
    out_weight,
    norm_gain,
    gate_weight,
    up_weight,
    down_weight,
    route_ids,
    route_weights,
):
    heads = attention(
        query_narrow, key_narrow, value_narrow, query_broad, key_broad, value_broad,
        narrow_query_gain, narrow_key_gain, broad_query_gain, broad_key_gain,
    )
    mixed = jnp.dot(heads, out_weight, preferred_element_type=jnp.float32)
    wide = (stream.astype(jnp.float32) + mixed).astype(jnp.bfloat16).astype(jnp.float32)
    normed = (
        wide * lax.rsqrt(jnp.mean(wide * wide, axis=-1, keepdims=True) + eps) * norm_gain
    ).astype(jnp.bfloat16)
    tokens_here, topk = route_ids.shape
    width_model = normed.shape[1]
    experts = lax.axis_size("sp")
    capacity = (2 * tokens_here * topk + experts - 1) // experts
    flat = route_ids.reshape(-1)
    hits = (flat[:, None] == jnp.arange(experts, dtype=jnp.int32)[None, :]).astype(jnp.int32)
    ranks = jnp.sum((jnp.cumsum(hits, axis=0) - 1) * hits, axis=1)
    slots = flat * capacity + ranks
    table = (jnp.arange(experts * capacity, dtype=jnp.int32)[:, None] == slots[None, :]).astype(
        jnp.bfloat16
    )
    table = jnp.sum(table.reshape(experts * capacity, tokens_here, topk), axis=2)
    sent = jnp.dot(table, normed, preferred_element_type=jnp.float32).astype(jnp.bfloat16)
    sent = sent.reshape(experts, capacity, width_model)
    piece = gather_directly(
        lax.all_to_all(sent, "sp", split_axis=0, concat_axis=0, tiled=True), "tp", 0
    )
    rows = piece.reshape(-1, piece.shape[-1])
    gate = jnp.dot(rows, gate_weight[0], preferred_element_type=jnp.float32)
    upper = jnp.dot(rows, up_weight[0], preferred_element_type=jnp.float32)
    hidden = (jax.nn.silu(gate) * upper).astype(jnp.bfloat16)
    partial_out = jnp.dot(hidden, down_weight[0], preferred_element_type=jnp.float32).astype(
        jnp.bfloat16
    )
    terms = lax.optimization_barrier(partial_out).astype(jnp.float32).reshape(piece.shape)
    summed = summed_on_arrival(terms.astype(jnp.bfloat16), "tp", 0).astype(jnp.bfloat16)
    back = lax.all_to_all(summed, "sp", split_axis=0, concat_axis=0, tiled=True)
    picked = jnp.take(back.reshape(experts * capacity, width_model), slots, axis=0)
    picked = picked.astype(jnp.float32).reshape(tokens_here, topk, width_model)
    routed = jnp.sum(picked * route_weights[..., None], axis=1)
    return (wide + routed).astype(jnp.bfloat16)


def solution(mesh):
    return jax.shard_map(
        local,
        mesh=mesh,
        in_specs=(
            P(("sp", "tp"), None),
            P("sp", "tp"),
            P("sp", "tp"),
            P("sp", "tp"),
            P("sp", "tp"),
            P("sp", "tp"),
            P("sp", "tp"),
            P(),
            P(),
            P(),
            P(),
            P(),
            P(),
            P("sp", None, "tp"),
            P("sp", None, "tp"),
            P("sp", "tp", None),
            P(("sp", "tp"), None),
            P(("sp", "tp"), None),
        ),
        out_specs=P(("sp", "tp"), None),
        check_vma=False,
    )
```

time: 638 us -> 237 us (0.37); the launches traced: 630 us -> 236 us
  matrix products: 254 us -> 19.5 us
  waiting for transfers between devices: 147 us -> 29.5 us
  Pallas kernels: 0 us -> 96.4 us
  other arithmetic: 101 us -> 13 us
  local copies, waits for them, and re-layouts: 44.2 us -> 15.4 us
  between operations: 13.8 us -> 0.14 us
    dot_general x33 -> x1, matrix products: 240 us -> 4.98 us  [local(): mixed = jnp.dot(heads, out_weight, preferred_element_type=jnp.float32)]
    all_gather x4 -> x0, waiting for transfers between devices: 116 us -> none  [the longest x1 63 us: local(): lax.all_gather(value_narrow, 'sp', axis=0, tiled=True)]
    pallas_call x0 -> x1, Pallas kernels: none -> 96.4 us  [attention(): pl.pallas_call(attention_kernel, out_shape=jax.ShapeDtypeStruct((128, 204...]
    reduce_sum x21 -> x0, other arithmetic: 81.5 us -> none  [the longest x16 80.2 us: attend_block(): total = total * shrink + jnp.sum(weights, axis=-1)]
    unnamed x33 -> x16, local copies, waits for them, and re-layouts: 23.1 us -> 6.01 us
    all_to_all x2 -> x1, blocking collectives: 16.6 us -> 11.9 us  [summed_on_arrival(): blocks = lax.all_to_all(cut_along(value, dim, size), axis, 0, 0, tiled=True)]
  transfers between devices with their start and end apart: 5 -> 1, of which waited for: 3 -> 1; matrix products, arithmetic and copies ran while one was open for 40% -> 0% of each run, Pallas kernels for 0% -> 0%
where the time goes in v1:
time: 237 us; the launch traced here: 236 us
  Pallas kernels  96.4 us (41%)
  blocking collectives  56 us (24%)
  waiting for transfers between devices  29.5 us (12%)
  matrix products  19.5 us (8%)
  local copies, waits for them, and re-layouts  15.4 us (6%)
  other arithmetic  13 us (5%)
  starting transfers between devices  6.15 us (3%)
    pallas_call x1, Pallas kernels, attention(): pl.pallas_call(attention_kernel, out_shape=jax.ShapeDtypeStruct((128, 204...  96.4 us
    all_to_all x1, blocking collectives, local(): lax.all_to_all(sent, 'sp', split_axis=0, concat_axis=0, tiled=True)  36.9 us
    all_to_all x1, waiting for transfers between devices, local(): back = lax.all_to_all(summed, 'sp', split_axis=0, concat_axis=0, tiled=True)  29.5 us
    all_to_all x1, blocking collectives, summed_on_arrival(): blocks = lax.all_to_all(cut_along(value, dim, size), axis, 0, 0, tiled=True)  11.9 us
    dot_general x1, matrix products, local(): jnp.dot(hidden, down_weight[0], preferred_element_type=jnp.float32)  10.1 us
    gather x2, local copies, waits for them, and re-layouts, local(): jnp.take(back.reshape(experts * capacity, width_model), slots, axis=0)  7.75 us
    all_to_all x1, blocking collectives, copy_for_each(): lax.all_to_all(jnp.broadcast_to(value[None], (size, *value.shape)), axis,...  7.23 us
    all_to_all x1, starting transfers between devices, local(): back = lax.all_to_all(summed, 'sp', split_axis=0, concat_axis=0, tiled=True)  6.15 us
  transfers between devices with their start and end apart: 1, of which 1 were waited for; matrix products, arithmetic and copies ran while one was open for 0% of the time, Pallas kernels for 0%

profile of v1, /device:TPU:0, one launch (start us, length us, event | category | flops | bytes accessed | tf_op | source)
XLA Modules:
  0.0 236.1 jit_solution(17700617861223087710)
XLA Ops:
  0.0 0.9 copy.42
  1.2 0.6 reduce-window.6
  1.8 0.2 slice_reduce_fusion
  2.2 0.1 reduce_sum.56
  2.4 0.7 compare_and_fusion
  3.2 1.5 copy.40.kn_ref
  4.7 1.5 copy.41.vn_ref
  6.1 96.4 %attention.1 = bf16[128,2048]{1,0:T(8,128)(2,1)} custom-call(bf16[256,512]{1,0:T(8,128)(2,1)} %qn_ref.1, bf16[256,64]{1,0:T(8,128)(2,1)} %copy.40.kn_ref, bf16[256,64]{1,0:T(8,128)(2,1)} %copy.41.vn_ref, bf16[256,512]{1,0:T(8,128)(2,1)} %qb_ref.1, bf16[256,128]{1,0:T(8,128)(2,1)} %kb_ref.1, bf16[256,128]{1,0:T(8,128)(2,1)} %vb_ref.1, f32[1,64]{1,0:T(1,128)} %bitcast.49, ...), custom_call_target="tpu_custom_call" | custom-call | tf_op jit(solution)/shard_map/attention/pallas_call | solution.py:333
  102.6 5.0 %multiply_reduce_fusion.1 = (f32[128]{0:T(128)S(1)}, f32[128,2048]{1,0:T(8,128)S(1)}) fusion(bf16[128,2048]{1,0:T(8,128)(2,1)} %attention.1, bf16[2048,2048]{1,0:T(8,128)(2,1)} %param.30, bf16[128,2048]{1,0:T(8,128)(2,1)} %param.19), kind=kOutput, calls=%fused_computation.17 | convolution fusion | flops 1075314560 | bytes 10486272 | tf_op jit(solution)/shard_map/dot_general | solution.py:416
  107.6 0.8 fusion
  108.4 36.9 %all_to_all.20 = bf16[64,8,2048]{2,1,0:T(8,128)(2,1)S(1)} all-to-all(bf16[64,8,2048]{2,1,0:T(8,128)(2,1)S(1)} %fusion), channel_id=1, replica_groups=mesh['sp'=64,'tp'=2] {'sp'}, dimensions={0} | all-to-all | bytes 4194304 | tf_op jit(solution)/shard_map/all_to_all | solution.py:436
  145.3 0.5 broadcast_in_dim.10
  145.9 7.2 %all_to_all.21 = bf16[2,64,8,2048]{3,2,1,0:T(8,128)(2,1)S(1)} all-to-all(bf16[2,64,8,2048]{3,2,1,0:T(8,128)(2,1)S(1)} %broadcast_in_dim.10), channel_id=1, replica_groups=mesh['sp'=64,'tp'=2] {'tp'}, dimensions={0} | all-to-all | bytes 8388608 | tf_op jit(solution)/shard_map/all_to_all | solution.py:383
  153.1 2.0 copy-done.1
  155.1 3.7 %fusion.4 = f32[1024,512]{1,0:T(8,128)} fusion(bf16[1024,2048]{1,0:T(8,128)(2,1)S(1)} %bitcast.44, bf16[1,2048,512]{2,1,0:T(8,128)(2,1)S(1)} %copy-done.5), kind=kOutput, calls=%fused_computation.8 | convolution fusion | flops 2147483648 | bytes 8388608 | tf_op jit(solution)/shard_map/dot_general | solution.py:440
  158.8 10.1 %convolution_convert_fusion = bf16[1024,2048]{1,0:T(8,128)(2,1)} fusion(bf16[1,512,2048]{2,1,0:T(8,128)(2,1)S(1)} %copy-done, f32[1024,512]{1,0:T(8,128)} %fusion.4, bf16[1024,2048]{1,0:T(8,128)(2,1)} %bitcast.45, bf16[1,2048,512]{2,1,0:T(8,128)(2,1)} %param.32), kind=kOutput, calls=%fused_computation.1 | convolution fusion | flops 4300210176 | bytes 14680064 | tf_op jit(solution)/shard_map/dot_general | solution.py:442
  168.8 11.9 %all_to_all.22 = bf16[2,64,8,2048]{3,2,1,0:T(8,128)(2,1)} all-to-all(bf16[2,64,8,2048]{3,2,1,0:T(8,128)(2,1)} %bitcast.46), channel_id=1, replica_groups=mesh['sp'=64,'tp'=2] {'tp'}, dimensions={0} | all-to-all | bytes 8388608 | tf_op jit(solution)/shard_map/all_to_all | solution.py:371
  180.7 5.1 %reduce_sum.59 = bf16[64,8,2048]{2,1,0:T(8,128)(2,1)} reduce(bf16[2,64,8,2048]{3,2,1,0:T(8,128)(2,1)} %all_to_all.22, bf16[]{:T(256)} %constant.35.clone.1), dimensions={0}, to_apply=%region_5.6 | reduce | flops 1048576 | bytes 6291458 | tf_op jit(solution)/shard_map/reduce_sum | solution.py:372
  185.8 6.2 %all-to-all-start.3 = ((bf16[64,8,2048]{2,1,0:T(8,128)(2,1)}), bf16[64,8,2048]{2,1,0:T(8,128)(2,1)}, u32[]{:S(2)}, u32[]{:S(2)}) async-start(bf16[64,8,2048]{2,1,0:T(8,128)(2,1)} %reduce_sum.59), calls=%async_computation.3 | async-start | bytes 4194304 | tf_op jit(solution)/shard_map/all_to_all | solution.py:447
  192.5 29.5 %all-to-all-done.3 = bf16[64,8,2048]{2,1,0:T(8,128)(2,1)} async-done(((bf16[64,8,2048]{2,1,0:T(8,128)(2,1)}), bf16[64,8,2048]{2,1,0:T(8,128)(2,1)}, u32[]{:S(2)}, u32[]{:S(2)}) %all-to-all-start.3) | async-done | bytes 2097184 | tf_op jit(solution)/shard_map/all_to_all | solution.py:447
  222.0 5.2 %gather_fusion = bf16[256,2048]{1,0:T(8,128)(2,1)} fusion(bf16[512,2048]{1,0:T(8,128)(2,1)} %bitcast.11, s32[1024]{0:T(1024)S(1)} %pad_clamp_fusion), kind=kCustom, calls=%fused_computation | custom fusion | bytes 2098176 | tf_op jit(solution)/shard_map/jit(_take)/gather | solution.py:448
  227.2 2.5 %gather.7 = bf16[128,2,2048]{2,1,0:T(2,128)(2,1)} reshape(bf16[256,2048]{1,0:T(8,128)(2,1)} %gather_fusion) | data formatting | bytes 2097152 | tf_op jit(solution)/shard_map/jit(_take)/gather | solution.py:448
  229.7 5.5 %multiply_reduce_fusion = f32[128,2048]{1,0:T(8,128)S(1)} fusion(bf16[128,2,2048]{2,1,0:T(2,128)(2,1)} %gather.7, pred[128,2]{1,0:T(8,128)(4,1)S(1)} %copy.46, f32[128,2]{1,0:T(8,128)S(1)} %copy.48), kind=kLoop, calls=%fused_computation.12 | loop fusion | flops 1835008 | bytes 2098432 | tf_op jit(solution)/shard_map/reduce_sum | solution.py:450
  235.2 0.9 add_convert_fusion
  (27 shorter events, 1.1 us)
Async XLA Ops:
  0.0 158.8 %copy-start = (bf16[1,512,2048]{2,1,0:T(8,128)(2,1)S(1)}, bf16[1,512,2048]{2,1,0:T(8,128)(2,1)}, u32[]{:S(2)}) copy-start(bf16[1,512,2048]{2,1,0:T(8,128)(2,1)} %param.34) | copy-start | bytes 6291460
  102.6 5.0 %copy-start.3 = (f32[2048]{0:T(1024)S(1)}, f32[2048]{0:T(1024)}, u32[]{:S(2)}) copy-start(f32[2048]{0:T(1024)} %param.31) | copy-start | bytes 24580
  145.8 9.2 %copy-start.5 = (bf16[1,2048,512]{2,1,0:T(8,128)(2,1)S(1)}, bf16[1,2048,512]{2,1,0:T(8,128)(2,1)}, u32[]{:S(2)}) copy-start(bf16[1,2048,512]{2,1,0:T(8,128)(2,1)} %param.33) | copy-start | bytes 6291460
  153.1 2.0 copy-start.1
  185.8 6.2 %copy-start.2 = (s32[128,2]{0,1:T(2,128)S(1)}, s32[128,2]{0,1:T(2,128)}, u32[]{:S(2)}) copy-start(s32[128,2]{0,1:T(2,128)} %param.35) | copy-start | bytes 3076
  185.8 6.6 %copy-start.4 = (f32[128,2]{0,1:T(2,128)S(1)}, f32[128,2]{0,1:T(2,128)}, u32[]{:S(2)}) copy-start(f32[128,2]{0,1:T(2,128)} %param.36) | copy-start | bytes 3076
  185.8 36.2 %all-to-all-start.3 = ((bf16[64,8,2048]{2,1,0:T(8,128)(2,1)}), bf16[64,8,2048]{2,1,0:T(8,128)(2,1)}, u32[]{:S(2)}, u32[]{:S(2)}) async-start(bf16[64,8,2048]{2,1,0:T(8,128)(2,1)} %reduce_sum.59), calls=%async_computation.3 | async-start | bytes 4194304 | tf_op jit(solution)/shard_map/all_to_all | solution.py:447

commit v2 on v1

--- a/solution.py
+++ b/solution.py
@@ -20,6 +20,26 @@
 OFFSETS = (0, -1, 1, 2)
 
 
+def far_first():
+    offs = [(a, b, c) for a in range(4) for b in range(4) for c in range(4) if a + b + c > 0]
+    seen, groups = set(), []
+    for o in offs:
+        if o in seen:
+            continue
+        orbit = []
+        for r in (o, (o[1], o[2], o[0]), (o[2], o[0], o[1])):
+            for s in (r, tuple((-v) % 4 for v in r)):
+                if s not in orbit:
+                    orbit.append(s)
+        seen.update(orbit)
+        groups.append(orbit)
+    groups.sort(key=lambda g: -sum(min(v, 4 - v) for v in g[0]))
+    return [o for g in groups for o in g]
+
+
+PEERS = far_first()
+
+
 def sem_index(piece, phase, item, way):
     base = (0, 4, 20)[phase]
     return piece * 36 + base + item * 4 + way
@@ -55,10 +75,14 @@
     return jnp.concatenate([col, col], axis=1)
 
 
-def attention_kernel(
+def layer_kernel(
     qn_ref, kn_ref, vn_ref, qb_ref, kb_ref, vb_ref, gqn_ref, gkn_ref, gqb_ref, gkb_ref, inv_ref,
+    stream_ref, ngain_ref, ids_ref, rw_ref, ow_hbm, gw_hbm, uw_hbm, dw_hbm,
     out_ref,
-    kv, qna, qnb, qbt, s_scr, st_m, st_l, on, ob, heads, send_sem, recv_sem, tp_send, tp_recv,
+    kv, qna, qnb, qbt, s_scr, st_m, st_l, on, ob, heads, full, ow, gw, uw, dw, wide, normed,
+    table, comb, sent, got, got2, part_a, part_b, part_c, ret, back,
+    send_sem, recv_sem, tp_send, tp_recv, load_sem, d_send, d_recv, r_send, r_recv,
+    f_send, f_recv, p_send, p_recv,
 ):
     sp = lax.axis_index("sp")
     tp = lax.axis_index("tp")
@@ -69,11 +93,23 @@
         at[dim] = (at[dim] + step + 4) % 4
         return (at[0] * 4 + at[1]) * 4 + at[2]
 
+    def chip_at(offset, sign):
+        at = [(me[d] + sign * offset[d] + 4) % 4 for d in range(3)]
+        return (at[0] * 4 + at[1]) * 4 + at[2]
+
     barrier = pltpu.get_barrier_semaphore()
-    for dim in range(3):
-        for step in (1, -1):
-            pl.semaphore_signal(barrier, inc=1, device_id=(neighbour(dim, step), tp), device_id_type=MESH)
+    for o in PEERS:
+        pl.semaphore_signal(barrier, inc=1, device_id=(chip_at(o, 1), tp), device_id_type=MESH)
     pl.semaphore_signal(barrier, inc=1, device_id=(sp, 1 - tp), device_id_type=MESH)
+
+    loads = [
+        pltpu.make_async_copy(ow_hbm, ow, load_sem.at[0]),
+        pltpu.make_async_copy(gw_hbm.at[0], gw, load_sem.at[1]),
+        pltpu.make_async_copy(uw_hbm.at[0], uw, load_sem.at[2]),
+        pltpu.make_async_copy(dw_hbm.at[0], dw, load_sem.at[3]),
+    ]
+    for load in loads:
+        load.start()
 
     lane = lax.broadcasted_iota(jnp.int32, (8, 256), 1)
     rows_of = ((lane // 128) + sp * 2).astype(F32)
@@ -88,18 +124,17 @@
     tab_n = tables(0, 16)
     tab_b = tables(16, 32)
 
-    kvn = jnp.concatenate([kn_ref[...].astype(F32), vn_ref[...].astype(F32)], axis=1).T
-    kt = rotate(normed_rows(kvn[:64], gain_column(gkn_ref)[:64]), *tab_n)
-    vt = kvn[64:]
+    kt = rotate(normed_rows(kn_ref[...].astype(F32), gain_column(gkn_ref)[:64]), *tab_n)
+    vt = vn_ref[...]
     here = kv.at[me[0], me[1], me[2]]
     here[0:128, :] = jnp.concatenate([kt[:, :128], kt[:, 128:]], axis=0).T.astype(BF)
-    here[128:256, :] = jnp.concatenate([vt[:, :128], vt[:, 128:]], axis=0).astype(BF)
+    here[128:256, :] = jnp.concatenate([vt[:, :128], vt[:, 128:]], axis=0)
     kbt = rotate(normed_rows(kb_ref[...].astype(F32).T, gain_column(gkb_ref)), *tab_b)
     here[256:512, :] = kbt.T.astype(BF)
     vbt = vb_ref[...].astype(F32).T
     here[512:768, :] = jnp.concatenate([vbt[:, :128], vbt[:, 128:]], axis=0).astype(BF)
 
-    pl.semaphore_wait(barrier, 7)
+    pl.semaphore_wait(barrier, 64)
 
     def part(piece, phase, item, way, mine):
         order = ORDERS[piece]
@@ -163,6 +198,22 @@
         hi = q.astype(BF)
         lo = (q - hi.astype(F32)).astype(BF)
         qbt[h] = jnp.concatenate([hi, lo], axis=0)
+
+    slot = lax.broadcasted_iota(jnp.int32, (512, 128), 0)
+    expert = slot // 8
+    ids = ids_ref[...]
+    first = expert == ids[0:1]
+    second_ = expert == ids[1:2]
+    hits = jnp.where(jnp.logical_or(first, second_), 1.0, 0.0)
+    before = lax.broadcasted_iota(jnp.int32, (128, 128), 0) < lax.broadcasted_iota(jnp.int32, (128, 128), 1)
+    ranks = jnp.dot(hits.astype(BF), jnp.where(before, 1.0, 0.0).astype(BF), preferred_element_type=F32)
+    chosen = jnp.where(ranks == (slot % 8).astype(F32), hits, 0.0)
+    table[...] = chosen.astype(BF)
+    rw = rw_ref[...]
+    weight = (chosen * (jnp.where(first, rw[0:1], 0.0) + jnp.where(second_, rw[1:2], 0.0))).T
+    weight_hi = weight.astype(BF)
+    comb[:, 0:512] = weight_hi
+    comb[:, 512:1024] = (weight - weight_hi.astype(F32)).astype(BF)
 
     st_m[...] = jnp.full(st_m.shape, -1e30, F32)
     st_l[...] = jnp.zeros(st_l.shape, F32)
@@ -307,33 +358,133 @@
     for g in range(2):
         place = pl.ds(pl.multiple_of(g * 1024 + tp * 512, 128), 512)
         swap = pltpu.make_async_remote_copy(
-            src_ref=heads.at[other, pl.ds(g * 512, 512)], dst_ref=out_ref.at[:, place],
+            src_ref=heads.at[other, pl.ds(g * 512, 512)], dst_ref=full.at[:, place],
             send_sem=tp_send.at[g], recv_sem=tp_recv.at[g], device_id=(sp, 1 - tp), device_id_type=MESH,
         )
         swap.start()
         swaps.append(swap)
-        out_ref[:, place] = heads[mine, pl.ds(g * 512, 512)]
+        full[:, place] = heads[mine, pl.ds(g * 512, 512)]
+    for g in range(2):
+        place = pl.ds(pl.multiple_of(g * 1024 + (1 - tp) * 512, 128), 512)
+        pltpu.make_async_remote_copy(
+            src_ref=heads.at[other, pl.ds(g * 512, 512)], dst_ref=full.at[:, place],
+            send_sem=tp_send.at[g], recv_sem=tp_recv.at[g], device_id=(sp, 1 - tp), device_id_type=MESH,
+        ).wait_recv()
+        swaps[g].wait_send()
+
+    for load in loads:
+        load.wait()
+    squares = jnp.zeros((128, 128), F32)
+    for b in range(4):
+        cols = slice(b * 512, b * 512 + 512)
+        m = jnp.dot(full[...], ow[:, cols], preferred_element_type=F32)
+        m = (stream_ref[:, cols].astype(F32) + m).astype(BF)
+        wide[:, cols] = m
+        m = m.astype(F32)
+        m = m * m
+        squares = squares + ((m[:, 0:128] + m[:, 128:256]) + (m[:, 256:384] + m[:, 384:512]))
+    scale = lax.rsqrt(jnp.sum(squares, axis=1, keepdims=True) / 2048 + eps)
+    for b in range(4):
+        cols = slice(b * 512, b * 512 + 512)
+        normed[:, cols] = (wide[:, cols].astype(F32) * scale * ngain_ref[:, cols]).astype(BF)
+
+    for b in range(8):
+        cols = slice(b * 256, b * 256 + 256)
+        rows = jnp.dot(table[...], normed[:, cols], preferred_element_type=F32)
+        sent[:, :, cols] = rows.reshape(64, 8, 256).astype(BF)
+
+    def dispatch(n):
+        to = chip_at(PEERS[n], 1)
+        return pltpu.make_async_remote_copy(
+            src_ref=sent.at[to], dst_ref=got.at[n], send_sem=d_send.at[n], recv_sem=d_recv.at[n],
+            device_id=(to, tp), device_id_type=MESH,
+        )
+
+    def giveback(n):
+        to = chip_at(PEERS[n], -1)
+        return pltpu.make_async_remote_copy(
+            src_ref=ret.at[n], dst_ref=back.at[sp], send_sem=r_send.at[n], recv_sem=r_recv.at[n],
+            device_id=(to, tp), device_id_type=MESH,
+        )
+
+    def given(n):
+        at = chip_at(PEERS[n], 1)
+        return pltpu.make_async_remote_copy(
+            src_ref=ret.at[n], dst_ref=back.at[at], send_sem=r_send.at[n], recv_sem=r_recv.at[n],
+            device_id=(at, tp), device_id_type=MESH,
+        )
+
+    for n in range(63):
+        dispatch(n).start()
+    got[63] = sent[sp]
+
+    def forward(c):
+        rows = pl.ds(c * 16, 16)
+        return pltpu.make_async_remote_copy(
+            src_ref=got.at[rows], dst_ref=got2.at[rows], send_sem=f_send.at[c], recv_sem=f_recv.at[c],
+            device_id=(sp, 1 - tp), device_id_type=MESH,
+        )
+
+    def partial(c):
+        return pltpu.make_async_remote_copy(
+            src_ref=part_b.at[c], dst_ref=part_c.at[c], send_sem=p_send.at[c], recv_sem=p_recv.at[c],
+            device_id=(sp, 1 - tp), device_id_type=MESH,
+        )
+
+    for c in range(4):
+        members = [n for n in range(c * 16, c * 16 + 16) if n < 63]
+        for n in members:
+            dispatch(n).wait_recv()
+        forward(c).start()
+        forward(c).wait_recv()
+        rows = jnp.concatenate(
+            [got[c * 16 : c * 16 + 16].reshape(128, 2048), got2[c * 16 : c * 16 + 16].reshape(128, 2048)], axis=0
+        )
+        gate = jnp.dot(rows, gw[...], preferred_element_type=F32)
+        upper = jnp.dot(rows, uw[...], preferred_element_type=F32)
+        hidden = (gate / (1.0 + jnp.exp(-gate)) * upper).astype(BF)
+        for b in range(4):
+            cols = slice(b * 512, b * 512 + 512)
+            piece = jnp.dot(hidden, dw[:, cols], preferred_element_type=F32).astype(BF)
+            part_a[:, cols] = piece[:128]
+            part_b[c, :, cols] = piece[128:]
+        partial(c).start()
+        partial(c).wait_recv()
+        total = (part_a[...].astype(F32) + part_c[c].astype(F32)).astype(BF)
+        ret[c * 16 : c * 16 + 16] = total.reshape(16, 8, 2048)
+        for n in members:
+            giveback(n).start()
+    back[sp] = ret[63]
+    for n in range(63):
+        given(n).wait_recv()
+    rows = back[...].reshape(512, 2048)
+    for b in range(4):
+        cols = slice(b * 512, b * 512 + 512)
+        piece = rows[:, cols]
+        routed = jnp.dot(comb[...], jnp.concatenate([piece, piece], axis=0), preferred_element_type=F32)
+        out_ref[:, cols] = (wide[:, cols].astype(F32) + routed).astype(BF)
+    for n in range(63):
+        dispatch(n).wait_send()
+        giveback(n).wait_send()
+    for c in range(4):
+        forward(c).wait_send()
+        partial(c).wait_send()
     for p in pieces:
         for phase in range(3):
             for item in range(1 if phase == 0 else 4):
                 for way in range(4):
                     copy_of(p, phase, item, way, True).wait_send()
-    for g in range(2):
-        place = pl.ds(pl.multiple_of(g * 1024 + (1 - tp) * 512, 128), 512)
-        pltpu.make_async_remote_copy(
-            src_ref=heads.at[other, pl.ds(g * 512, 512)], dst_ref=out_ref.at[:, place],
-            send_sem=tp_send.at[g], recv_sem=tp_recv.at[g], device_id=(sp, 1 - tp), device_id_type=MESH,
-        ).wait_recv()
-        swaps[g].wait_send()
-
-
-def attention(qn, kn, vn, qb, kb, vb, gqn, gkn, gqb, gkb):
+
+
+def layer(
+    stream, qn, kn, vn, qb, kb, vb, gqn, gkn, gqb, gkb, ow, ngain, gw, uw, dw, route_ids, route_weights
+):
     inv = jnp.asarray(inverse_table())
     vm = pl.BlockSpec(memory_space=pltpu.VMEM)
     return pl.pallas_call(
-        attention_kernel,
+        layer_kernel,
         out_shape=jax.ShapeDtypeStruct((128, 2048), BF),
-        in_specs=[vm] * 11,
+        in_specs=[vm] * 15 + [pl.BlockSpec(memory_space=pl.ANY)] * 4,
         out_specs=vm,
         scratch_shapes=[
             pltpu.VMEM((4, 4, 4, 768, 128), BF),
@@ -346,114 +497,51 @@
             pltpu.VMEM((8, 64, 256), F32),
             pltpu.VMEM((4, 128, 256), F32),
             pltpu.VMEM((256, 1024), BF),
+            pltpu.VMEM((128, 2048), BF),
+            pltpu.VMEM((2048, 2048), BF),
+            pltpu.VMEM((2048, 512), BF),
+            pltpu.VMEM((2048, 512), BF),
+            pltpu.VMEM((512, 2048), BF),
+            pltpu.VMEM((128, 2048), BF),
+            pltpu.VMEM((128, 2048), BF),
+            pltpu.VMEM((512, 128), BF),
+            pltpu.VMEM((128, 1024), BF),
+            pltpu.VMEM((64, 8, 2048), BF),
+            pltpu.VMEM((64, 8, 2048), BF),
+            pltpu.VMEM((64, 8, 2048), BF),
+            pltpu.VMEM((128, 2048), BF),
+            pltpu.VMEM((4, 128, 2048), BF),
+            pltpu.VMEM((4, 128, 2048), BF),
+            pltpu.VMEM((64, 8, 2048), BF),
+            pltpu.VMEM((64, 8, 2048), BF),
             pltpu.SemaphoreType.DMA((108,)),
             pltpu.SemaphoreType.DMA((108,)),
             pltpu.SemaphoreType.DMA((2,)),
             pltpu.SemaphoreType.DMA((2,)),
+            pltpu.SemaphoreType.DMA((4,)),
+            pltpu.SemaphoreType.DMA((63,)),
+            pltpu.SemaphoreType.DMA((63,)),
+            pltpu.SemaphoreType.DMA((63,)),
+            pltpu.SemaphoreType.DMA((63,)),
+            pltpu.SemaphoreType.DMA((4,)),
+            pltpu.SemaphoreType.DMA((4,)),
+            pltpu.SemaphoreType.DMA((4,)),
+            pltpu.SemaphoreType.DMA((4,)),
         ],
         compiler_params=pltpu.CompilerParams(
-            collective_id=0, has_side_effects=True, vmem_limit_bytes=60 * 1024 * 1024
+            collective_id=0, has_side_effects=True, vmem_limit_bytes=67043328
         ),
-        name="attention",
+        name="layer",
     )(
-        qn, kn, vn, qb, kb, vb,
+        qn, kn.T, vn.T, qb, kb, vb,
         gqn.reshape(1, -1), gkn.reshape(1, -1), gqb.reshape(1, -1), gkb.reshape(1, -1), inv,
+        stream, ngain.reshape(1, -1), route_ids.T, route_weights.T, ow, gw, uw, dw,
     )
-
-
-def cut_along(value, dim, size):
-    before, after = (value.shape[:dim], value.shape[dim + 1 :])
-    return jnp.moveaxis(value.reshape(*before, size, -1, *after), dim, 0)
-
-
-def summed_on_arrival(value, axis, dim):
-    size = lax.axis_size(axis)
-    blocks = lax.all_to_all(cut_along(value, dim, size), axis, 0, 0, tiled=True)
-    return jnp.sum(blocks.astype(jnp.float32), axis=0)
-
-
-def joined_along(blocks, dim):
-    shape = list(blocks.shape[1:])
-    shape[dim] *= blocks.shape[0]
-    return jnp.moveaxis(blocks, 0, dim).reshape(shape)
-
-
-def copy_for_each(value, axis):
-    size = lax.axis_size(axis)
-    return lax.all_to_all(
-        jnp.broadcast_to(value[None], (size, *value.shape)), axis, 0, 0, tiled=True
-    )
-
-
-def gather_directly(value, axis, dim):
-    return joined_along(copy_for_each(value, axis), dim)
-
-
-def local(
-    stream,
-    query_narrow,
-    key_narrow,
-    value_narrow,
-    query_broad,
-    key_broad,
-    value_broad,
-    narrow_query_gain,
-    narrow_key_gain,
-    broad_query_gain,
-    broad_key_gain,
-    out_weight,
-    norm_gain,
-    gate_weight,
-    up_weight,
-    down_weight,
-    route_ids,
-    route_weights,
-):
-    heads = attention(
-        query_narrow, key_narrow, value_narrow, query_broad, key_broad, value_broad,
-        narrow_query_gain, narrow_key_gain, broad_query_gain, broad_key_gain,
-    )
-    mixed = jnp.dot(heads, out_weight, preferred_element_type=jnp.float32)
-    wide = (stream.astype(jnp.float32) + mixed).astype(jnp.bfloat16).astype(jnp.float32)
-    normed = (
-        wide * lax.rsqrt(jnp.mean(wide * wide, axis=-1, keepdims=True) + eps) * norm_gain
-    ).astype(jnp.bfloat16)
-    tokens_here, topk = route_ids.shape
-    width_model = normed.shape[1]
-    experts = lax.axis_size("sp")
-    capacity = (2 * tokens_here * topk + experts - 1) // experts
-    flat = route_ids.reshape(-1)
-    hits = (flat[:, None] == jnp.arange(experts, dtype=jnp.int32)[None, :]).astype(jnp.int32)
-    ranks = jnp.sum((jnp.cumsum(hits, axis=0) - 1) * hits, axis=1)
-    slots = flat * capacity + ranks
-    table = (jnp.arange(experts * capacity, dtype=jnp.int32)[:, None] == slots[None, :]).astype(
-        jnp.bfloat16
-    )
-    table = jnp.sum(table.reshape(experts * capacity, tokens_here, topk), axis=2)
-    sent = jnp.dot(table, normed, preferred_element_type=jnp.float32).astype(jnp.bfloat16)
-    sent = sent.reshape(experts, capacity, width_model)
-    piece = gather_directly(
-        lax.all_to_all(sent, "sp", split_axis=0, concat_axis=0, tiled=True), "tp", 0
-    )
-    rows = piece.reshape(-1, piece.shape[-1])
-    gate = jnp.dot(rows, gate_weight[0], preferred_element_type=jnp.float32)
-    upper = jnp.dot(rows, up_weight[0], preferred_element_type=jnp.float32)
-    hidden = (jax.nn.silu(gate) * upper).astype(jnp.bfloat16)
-    partial_out = jnp.dot(hidden, down_weight[0], preferred_element_type=jnp.float32).astype(
-        jnp.bfloat16
-    )
-    terms = lax.optimization_barrier(partial_out).astype(jnp.float32).reshape(piece.shape)
-    summed = summed_on_arrival(terms.astype(jnp.bfloat16), "tp", 0).astype(jnp.bfloat16)
-    back = lax.all_to_all(summed, "sp", split_axis=0, concat_axis=0, tiled=True)
-    picked = jnp.take(back.reshape(experts * capacity, width_model), slots, axis=0)
-    picked = picked.astype(jnp.float32).reshape(tokens_here, topk, width_model)
-    routed = jnp.sum(picked * route_weights[..., None], axis=1)
-    return (wide + routed).astype(jnp.bfloat16)
 
 
 def solution(mesh):
     return jax.shard_map(
-        local,
+        layer,
         mesh=mesh,
         in_specs=(
             P(("sp", "tp"), None),

time: 237 us -> 158 us (0.67)
  Pallas kernels: 96.4 us -> 155 us
  blocking collectives: 56 us -> 0 us
  waiting for transfers between devices: 29.5 us -> 0 us
  matrix products: 19.5 us -> 0 us
  local copies, waits for them, and re-layouts: 15.4 us -> 1.88 us
  other arithmetic: 13 us -> 0 us
  starting transfers between devices: 6.15 us -> 0 us
    pallas_call x1, Pallas kernels: 96.4 us -> 155 us  [layer(): pl.pallas_call(layer_kernel, out_shape=jax.ShapeDtypeStruct((128, 2048),...]
    all_to_all x3 -> x0, blocking collectives: 56 us -> none  [the longest x1 36.9 us: local(): lax.all_to_all(sent, 'sp', split_axis=0, concat_axis=0, tiled=True)]
    all_to_all x1 -> x0, waiting for transfers between devices: 29.5 us -> none  [local(): back = lax.all_to_all(summed, 'sp', split_axis=0, concat_axis=0, tiled=True)]
    dot_general x4 -> x0, matrix products: 19.5 us -> none  [the longest x1 10.1 us: local(): jnp.dot(hidden, down_weight[0], preferred_element_type=jnp.float32)]
    reduce_sum x4 -> x0, other arithmetic: 10.7 us -> none  [the longest x1 5.47 us: local(): routed = jnp.sum(picked * route_weights[..., None], axis=1)]
    gather x2 -> x0, local copies, waits for them, and re-layouts: 7.75 us -> none  [local(): jnp.take(back.reshape(experts * capacity, width_model), slots, axis=0)]
    all_to_all x1 -> x0, starting transfers between devices: 6.15 us -> none  [local(): back = lax.all_to_all(summed, 'sp', split_axis=0, concat_axis=0, tiled=True)]
    unnamed x16 -> x1, local copies, waits for them, and re-layouts: 6.01 us -> 1.88 us
  transfers between devices with their start and end apart: 1 -> 0, of which waited for: 1 -> 0; matrix products, arithmetic and copies ran while one was open for 0% -> 0% of each run, Pallas kernels for 0% -> 0%
where the time goes in v2:
time: 158 us; the launch traced here: 157 us
  Pallas kernels  155 us (98%)
  local copies, waits for them, and re-layouts  1.88 us (1%)
    pallas_call x1, Pallas kernels, layer(): pl.pallas_call(layer_kernel, out_shape=jax.ShapeDtypeStruct((128, 2048),...  155 us

profile of v2, /device:TPU:0, one launch (start us, length us, event | category | flops | bytes accessed | tf_op | source)
XLA Modules:
  0.0 157.0 jit_solution(15838107207913842631)
XLA Ops:
  0.0 155.1 %layer.1 = bf16[128,2048]{1,0:T(8,128)(2,1)} custom-call(bf16[256,512]{1,0:T(8,128)(2,1)} %qn_ref.1, bf16[64,256]{1,0:T(8,128)(2,1)} %bitcast.9, bf16[64,256]{1,0:T(8,128)(2,1)} %bitcast.10, bf16[256,512]{1,0:T(8,128)(2,1)} %qb_ref.1, bf16[256,128]{1,0:T(8,128)(2,1)} %kb_ref.1, bf16[256,128]{1,0:T(8,128)(2,1)} %vb_ref.1, f32[1,64]{1,0:T(1,128)} %bitcast.14, ...), custom_call_target="tpu_custom_call" | custom-call | tf_op jit(solution)/shard_map/layer/pallas_call | solution.py:484
  155.1 1.9 %copy.21 = bf16[128,2048]{1,0:T(8,128)(2,1)} copy(bf16[128,2048]{1,0:T(8,128)(2,1)} %layer.1) | data formatting | bytes 1048576
